TPU v7x, 256 devices: a whole 4x4x8 slice. The times are simulated.
256 devices in a mesh: sp: 32 (over z, y), tp: 8 (over x, core).
Axes of the slice: x: 4, y: 4, z: 8, core: 2. Of those that a mesh axis runs over, the one named last changes fastest.
Arguments:
- tokens: bfloat16 [4, 16384, 2048], P(None, ('sp', 'tp')), may hold values from -6 to 6
- in_gain: float32 [2048], replicated, may hold values from 0.1 to 1.9
- query_weight: bfloat16 [2048, 1024], P(None, 'tp'), may hold values from -0.125 to 0.125
- key_weight: bfloat16 [2048, 1024], P(None, 'tp'), may hold values from -0.125 to 0.125
- value_weight: bfloat16 [2048, 1024], P(None, 'tp'), may hold values from -0.125 to 0.125
- gate_weight: bfloat16 [2048, 1024], P(None, 'tp'), may hold values from -0.125 to 0.125
- log_decay: float32 [8], P('tp'), may hold values from -0.034 to 0, as said below
- norm_gain: float32 [1024], P('tp'), may hold values from 0.1 to 1.9
- out_weight: bfloat16 [1024, 2048], replicated, may hold values from -0.1875 to 0.1875
- post_gain: float32 [2048], replicated, may hold values from 0.1 to 1.9
Outputs:
- mixed: bfloat16 [4, 16384, 2048], P(None, ('sp', 'tp'))
Inputs may be any that keep to these rules, and one draw needn't show every extreme that they name: `log_decay`: every entry is negative; some heads keep a tenth or more of their memory over 16384 positions, others lose most of it within 30 to 100 positions.
All inputs are finite; a program needn't handle non-finite values.
Results may differ from a plain program's by a relative error of at most 0.015.
Values may be sent and summed in bfloat16 or wider, within the bound.
A program may use at most 64 MiB of HBM per device.

v0:
```python
import jax
import jax.numpy as jnp
from jax import lax
from jax.sharding import Mesh
from jax.sharding import PartitionSpec as P

HEAD_DIM = 128
BLOCK = 128
SP = ("sp_0", "sp_1")
SP_TP = ("sp_0", "sp_1", "tp")
rms_eps = 1e-06
group_eps = 1e-05
rope_base = 10000.0


def neutral_like(shard, identity):
    return jax.tree.map(
        lambda part, zero: jnp.zeros_like(part) + jnp.asarray(zero, part.dtype), shard, identity
    )


def entering(shard, axes, combine, identity):
    before = start = neutral_like(shard, identity)
    running = shard
    for axis in reversed(axes):
        length, mine = (lax.axis_size(axis), lax.axis_index(axis))
        pieces = jax.tree.map(lambda part: lax.all_gather(part, axis), running)
        inside, running = (start, start)
        for k in range(length):
            passed = k < mine
            running = combine(running, jax.tree.map(lambda part: part[k], pieces))
            inside = jax.tree.map(lambda new, old: jnp.where(passed, new, old), running, inside)
        before = combine(inside, before)
    return before


def rotate(values, positions):
    half_dim = values.shape[-1] // 2
    inverse = rope_base ** (-jnp.arange(half_dim, dtype=jnp.float32) / half_dim)
    angles = positions.astype(jnp.float32)[:, None] * inverse[None, :]
    cosine = jnp.cos(angles)
    sine_part = jnp.sin(angles)
    first_half = values[..., :half_dim].astype(jnp.float32)
    second = values[..., half_dim:].astype(jnp.float32)
    return jnp.concatenate(
        [first_half * cosine - second * sine_part, first_half * sine_part + second * cosine],
        axis=-1,
    )


def local_pass(queries, key_rows, values, log_decay):
    seq_count, head_count, length, head_width = queries.shape
    block_count = length // BLOCK
    offsets = jnp.arange(BLOCK, dtype=jnp.float32)
    distance = offsets[:, None] - offsets[None, :]
    rate_col = log_decay[:, None, None]
    inside = jnp.where(distance >= 0, jnp.exp(rate_col * jnp.maximum(distance, 0.0)), 0.0)
    query_scale = jnp.exp(log_decay[:, None] * (offsets + 1.0))[..., None]
    key_scale = jnp.exp(log_decay[:, None] * (BLOCK - 1.0 - offsets))[..., None]
    block_decay = jnp.exp(log_decay * BLOCK)[:, None, None]

    def to_blocks(arr):
        return arr.reshape(seq_count, head_count, block_count, BLOCK, arr.shape[-1]).transpose(
            2, 0, 1, 3, 4
        )

    def advance(memory, inputs):
        q_block, k_block, v_block = inputs
        scores = jnp.einsum("shqd,shkd->shqk", q_block, k_block, preferred_element_type=jnp.float32)
        weights = (scores * inside).astype(jnp.bfloat16)
        within = jnp.einsum("shqk,shkv->shqv", weights, v_block, preferred_element_type=jnp.float32)
        carried = jnp.einsum("shqd,shdv->shqv", q_block.astype(jnp.float32) * query_scale, memory)
        k_scaled = (k_block.astype(jnp.float32) * key_scale).astype(jnp.bfloat16)
        memory = memory * block_decay + jnp.einsum(
            "shkd,shkv->shdv", k_scaled, v_block, preferred_element_type=jnp.float32
        )
        return (memory, within + carried)

    start_memory = jnp.zeros((seq_count, head_count, head_width, values.shape[-1]), jnp.float32)
    end_state, outputs = lax.scan(
        advance, start_memory, (to_blocks(queries), to_blocks(key_rows), to_blocks(values))
    )
    outputs = outputs.transpose(1, 2, 0, 3, 4).reshape(
        seq_count, head_count, length, values.shape[-1]
    )
    return (outputs, end_state)


def combine(earlier, later_part):
    return (
        earlier[0] * later_part[0],
        earlier[1] * later_part[0][None, :, None, None] + later_part[1],
    )


def read_out(carried, queries, partial_out, log_decay):
    length = queries.shape[2]
    read_scale = jnp.exp(log_decay[:, None] * (jnp.arange(length, dtype=jnp.float32) + 1.0))[
        ..., None
    ]
    return partial_out + jnp.einsum(
        "shld,shdv->shlv", queries.astype(jnp.float32) * read_scale, carried
    )


def body(
    tokens,
    in_gain,
    query_weight,
    key_weight,
    value_weight,
    gate_weight,
    log_decay,
    norm_gain,
    out_weight,
    post_gain,
):
    seq_count, rows_dev, model_width = tokens.shape
    tp_size = lax.axis_size("tp")
    local_width = query_weight.shape[1]
    head_count = local_width // HEAD_DIM
    stretch = rows_dev * tp_size
    tok_f32 = tokens.astype(jnp.float32)
    normed = (
        tok_f32 * lax.rsqrt(jnp.mean(tok_f32 * tok_f32, axis=-1, keepdims=True) + rms_eps) * in_gain
    ).astype(jnp.bfloat16)
    joined = jnp.concatenate([query_weight, key_weight, value_weight, gate_weight], axis=1)
    projected = jnp.einsum(
        "kux,xt->kut",
        lax.all_gather(normed, "tp", axis=1, tiled=True),
        joined,
        preferred_element_type=jnp.float32,
    ).astype(jnp.bfloat16)

    def heads_of(columns):
        return columns.reshape(seq_count, stretch, head_count, HEAD_DIM).transpose(0, 2, 1, 3)

    positions = lax.axis_index(SP) * stretch + jnp.arange(stretch, dtype=jnp.int32)
    queries = rotate(heads_of(projected[..., :local_width]), positions).astype(jnp.bfloat16)
    key_rows = (
        rotate(heads_of(projected[..., local_width : 2 * local_width]), positions)
        * HEAD_DIM ** (-0.5)
    ).astype(jnp.bfloat16)
    values = heads_of(projected[..., 2 * local_width : 3 * local_width])
    gating = projected[..., 3 * local_width :]
    partial_out, end_state = local_pass(queries, key_rows, values, log_decay)
    span_decay = jnp.exp(log_decay * stretch)
    carried = entering(
        (span_decay, end_state), SP, combine, (jnp.ones_like(span_decay), jnp.zeros_like(end_state))
    )[1]
    retained = read_out(carried, queries, partial_out, log_decay)
    center = jnp.mean(retained, axis=-1, keepdims=True)
    spread = jnp.mean(jnp.square(retained - center), axis=-1, keepdims=True)
    normal = (
        ((retained - center) * lax.rsqrt(spread + group_eps))
        .transpose(0, 2, 1, 3)
        .reshape(seq_count, stretch, local_width)
    )
    gated = (normal * norm_gain * jax.nn.silu(gating.astype(jnp.float32))).astype(jnp.bfloat16)
    premix = jnp.einsum(
        "hor,rn->hon",
        lax.all_to_all(gated, "tp", split_axis=1, concat_axis=2, tiled=True),
        out_weight,
        preferred_element_type=jnp.float32,
    )
    mixed = (
        premix * lax.rsqrt(jnp.mean(premix * premix, axis=-1, keepdims=True) + rms_eps) * post_gain
    )
    return mixed.astype(jnp.bfloat16)


def solution(mesh):
    torus = Mesh(mesh.devices.reshape(8, 4, mesh.shape["tp"]), ("sp_0", "sp_1", "tp"))
    return jax.shard_map(
        body,
        mesh=torus,
        in_specs=(
            P(None, SP_TP, None),
            P(),
            P(None, "tp"),
            P(None, "tp"),
            P(None, "tp"),
            P(None, "tp"),
            P("tp"),
            P("tp"),
            P(),
            P(),
        ),
        out_specs=P(None, SP_TP, None),
        check_vma=False,
    )
```

profile of v0, /device:TPU:1, one launch (start us, length us, event | category | flops | bytes accessed | tf_op | source)
XLA Modules:
  0.0 204.7 jit_solution(9332395953188734523)
XLA Ops:
  6.5 1.6 fusion.44
  8.1 2.6 %fusion.46 = bf16[4,64,2048]{2,1,0:T(8,128)(2,1)} fusion(bf16[4,64,2048]{2,1,0:T(8,128)(2,1)} %param.12, f32[2048]{0:T(1024)} %param.13, f32[4,64]{1,0:T(4,128)S(1)} %add_rsqrt_fusion.2), kind=kLoop, calls=%fused_computation.48 | loop fusion | flops 2097152 | bytes 2106368 | tf_op jit(solution)/shard_map/convert_element_type | solution.py:126
  13.5 53.8 %all-gather.7.cloned.1.call-done = bf16[4,512,2048]{2,1,0:T(8,128)(2,1)} async-done(((bf16[4,64,2048]{2,1,0:T(8,128)(2,1)}), bf16[4,512,2048]{2,1,0:T(8,128)(2,1)}) %all-gather.7.cloned.1.call-update) | async-done | bytes 8388624 | tf_op jit(solution)/shard_map/all_gather | solution.py:130
  67.3 9.5 %fusion.54 = bf16[4,512,512]{1,2,0:T(8,128)(2,1)S(1)} fusion(bf16[4,512,2048]{2,1,0:T(8,128)(2,1)} %all-gather.7.cloned.1.call-done, bf16[2048,128]{0,1:T(8,128)(2,1)S(1)} %copy.42, bf16[2048,128]{0,1:T(8,128)(2,1)S(1)} %copy.41, bf16[2048,128]{0,1:T(8,128)(2,1)S(1)} %copy.40, bf16[2048,128]{0,1:T(8,128)(2,1)S(1)} %copy.39), kind=kOutput, calls=%fused_computation.59 | convolution fusion | flops 4304404480 | bytes 12582912 | tf_op jit(solution)/shard_map/kux,xt->kut/dot_general | solution.py:128
  76.9 1.0 slice_bitcast_fusion
  80.3 1.3 copy.44
  81.6 1.2 reshape_transpose_reshape.3
  84.8 11.9 %while.15 = (s32[]{:T(128)}, f32[4,1,128,128]{3,2,0,1:T(8,128)S(1)}, f32[4,4,1,128,128]{4,3,1,2,0:T(8,128)}, f32[1]{0:T(128)}, bf16[4,4,1,128,128]{4,3,1,2,0:T(8...) while((s32[]{:T(128)}, ...), condition=%wide.region_2.3_spmd.clone.clone.clone, body=%wide.region_1.2_spmd.clone.clone.clone.sunk | while | flops 67977728 | bytes 2496632 | solution.py:80
  86.5 0.9 fusion.147
  89.5 0.9 fusion.147
  92.5 0.9 fusion.147
  95.5 0.9 fusion.147
  98.8 8.4 %all-reduce = f32[4]{0:T(128)S(1)} all-reduce(f32[4]{0:T(128)S(1)} %exponential_dynamic-update-slice_fusion), channel_id=2, replica_groups=mesh['sp_0'=8,'sp_1'=4,'tp'=8] {'sp_1'}, use_global_device_ids=true, to_apply=%add | all-reduce | flops 4 | bytes 32
  107.9 1.3 slice_multiply_fusion
  109.9 12.2 %all-gather.11.cloned.1.call-done = f32[16,1,128,128]{3,2,1,0:T(8,128)} async-done(((f32[4,1,128,128]{3,2,1,0:T(8,128)}), f32[16,1,128,128]{3,2,1,0:T(8,128)}) %all-gather.11.cloned.1.call-update) | async-done | bytes 1048592 | tf_op jit(solution)/shard_map/all_gather | solution.py:27
  122.0 3.8 %slice_add_fusion.8 = f32[4,1,128,128]{3,2,1,0:T(8,128)} fusion(f32[16,1,128,128]{3,2,1,0:T(8,128)} %all-gather.11.cloned.1.call-done, f32[]{:T(128)} %bitcast.20, f32[]{:T(128)} %bitcast.18, f32[16,1,128,128]{3,2,0,1:T(8,128)} %bitcast.197, f32[]{:T(128)} %bitcast.16, f32[]{:T(128)} %bitcast.13), kind=kLoop, calls=%fused_computation.109 | loop fusion | flops 458752 | bytes 1310736 | tf_op jit(solution)/shard_map/add | solution.py:92
  126.4 1.3 dynamic-update-slice.1
  127.7 13.9 %all-reduce.1 = f32[8]{0:T(128)S(1)} all-reduce(f32[8]{0:T(128)S(1)} %dynamic-update-slice.1), channel_id=3, replica_groups=mesh['sp_0'=8,'sp_1'=4,'tp'=8] {'sp_0'}, use_global_device_ids=true, to_apply=%add.1 | all-reduce | flops 8 | bytes 64
  146.3 18.7 %all-gather.9.cloned.1.call-done = f32[8,4,1,128,128]{4,3,2,1,0:T(8,128)} async-done(((f32[1,4,1,128,128]{4,3,2,1,0:T(8,128)}), f32[8,4,1,128,128]{4,3,2,1,0:T(8,128)}) %all-gather.9.cloned.1.call-update) | async-done | bytes 2097168 | tf_op jit(solution)/shard_map/all_gather | solution.py:27
  165.1 7.9 %fusion.128 = (f32[4,512]{1,0:T(4,128)S(1)}, f32[4,512,128]{1,2,0:T(8,128)S(1)}) fusion(f32[4,512,128]{1,2,0:T(8,128)S(1)} %reshape.499, f32[8,4,1,128,128]{4,3,1,2,0:T(8,128)} %bitcast.204, f32[4,1,128,128]{3,2,1,0:T(8,128)S(1)} %copy-done.4, f32[16,1,128,128]{3,2,0,1:T(8,128)S(1)} %bitcast.198, f32[16,1,128,128]{3,2,1,0:T(8,128)S(1)} %copy-done.3, ...), kind=kOutput, calls=%fused_computation.175 | convolution fusion | flops 71170048 | bytes 5777468 | tf_op jit(solution)/shard_map/shld,shdv->shlv/dot_general | solution.py:101
  173.2 1.5 fusion.62
  175.0 18.3 %all_to_all.18 = bf16[4,512,128]{2,0,1:T(4,128)(2,1)S(1)} all-to-all(bf16[4,512,128]{2,0,1:T(4,128)(2,1)S(1)} %copy.65), channel_id=1, replica_groups=mesh['sp_0'=8,'sp_1'=4,'tp'=8] {'tp'}, dimensions={1} | all-to-all | bytes 1048576 | tf_op jit(solution)/shard_map/all_to_all | solution.py:162
  193.4 3.6 %multiply_reduce_fusion = (f32[4,64]{1,0:T(4,128)S(1)}, f32[4,64,2048]{2,1,0:T(8,128)S(1)}) fusion(bf16[1024,2048]{1,0:T(8,128)(2,1)} %param.20, bf16[4,8,8,8,128]{4,3,2,1,0:T(8,128)(2,1)S(1)} %bitcast.203), kind=kOutput, calls=%fused_computation.58 | convolution fusion | flops 1074790144 | bytes 6816768 | tf_op jit(solution)/shard_map/hor,rn->hon/dot_general | solution.py:160
  197.0 1.2 multiply_convert_fusion.2
  (91 shorter events, 19.6 us)
Async XLA Ops:
  6.5 4.3 %copy-start.8 = (bf16[2048,128]{1,0:T(8,128)(2,1)S(1)}, bf16[2048,128]{1,0:T(8,128)(2,1)}, u32[]{:S(2)}) copy-start(bf16[2048,128]{1,0:T(8,128)(2,1)} %param.14) | copy-start | bytes 1572868
  6.5 60.8 %all-gather.7.cloned.1.call-start = ((), (), s32[]{:S(2)}) async-start(), calls=%async_computation.1 | async-start | bytes 9437184 | tf_op jit(solution)/shard_map/all_gather | solution.py:130
  8.1 3.0 %copy-start.9 = (bf16[2048,128]{1,0:T(8,128)(2,1)S(1)}, bf16[2048,128]{1,0:T(8,128)(2,1)}, u32[]{:S(2)}) copy-start(bf16[2048,128]{1,0:T(8,128)(2,1)} %param.15) | copy-start | bytes 1572868
  10.8 1.0 copy-start.10
  10.8 1.3 copy-start.11
  10.8 111.2 %all-gather.11.cloned.1.call-start = ((), (), s32[]{:S(2)}) async-start(), calls=%async_computation.3 | async-start | bytes 1310720 | tf_op jit(solution)/shard_map/all_gather | solution.py:27
  76.9 1.5 copy-start.2
  78.3 0.7 copy-start.6
  78.4 0.8 copy-start.7
  83.2 1.2 copy-start.1
  84.8 12.8 %copy-start.15 = (u32[256]{0:T(256)S(1)}, u32[256]{0:T(256)}, u32[]{:S(2)}) copy-start(u32[256]{0:T(256)} %constant.86) | copy-start | bytes 3076
  84.8 41.1 %copy-start.14 = (u32[256]{0:T(256)S(1)}, u32[256]{0:T(256)}, u32[]{:S(2)}) copy-start(u32[256]{0:T(256)} %constant.91) | copy-start | bytes 3076
  96.7 0.7 copy-start
  96.7 48.7 %copy-start.5 = (f32[4,4,1,128,128]{4,3,1,2,0:T(8,128)S(1)}, f32[4,4,1,128,128]{4,3,1,2,0:T(8,128)}, u32[]{:S(2)}) copy-start(f32[4,4,1,128,128]{4,3,1,2,0:T(8,128)} %get-tuple-element.58) | copy-start | bytes 3145732
  97.5 67.6 %all-gather.9.cloned.1.call-start = ((), (), s32[]{:S(2)}) async-start(), calls=%async_computation.2 | async-start | bytes 2359296 | tf_op jit(solution)/shard_map/all_gather | solution.py:27
  145.5 19.6 %copy-start.3 = (f32[16,1,128,128]{3,2,1,0:T(8,128)S(1)}, f32[16,1,128,128]{3,2,1,0:T(8,128)}, u32[]{:S(2)}) copy-start(f32[16,1,128,128]{3,2,1,0:T(8,128)} %all-gather.11.cloned.1.call-done) | copy-start | bytes 3145732
  145.5 19.6 %copy-start.4 = (f32[4,1,128,128]{3,2,1,0:T(8,128)S(1)}, f32[4,1,128,128]{3,2,1,0:T(8,128)}, u32[]{:S(2)}) copy-start(f32[4,1,128,128]{3,2,1,0:T(8,128)} %slice_add_fusion.8) | copy-start | bytes 786436
  165.1 8.1 %copy-start.13 = (f32[128]{0:T(128)S(1)}, f32[128]{0:T(128)}, u32[]{:S(2)}) copy-start(f32[128]{0:T(128)} %param.19) | copy-start | bytes 1540
  193.4 3.6 %copy-start.12 = (f32[2048]{0:T(1024)S(1)}, f32[2048]{0:T(1024)}, u32[]{:S(2)}) copy-start(f32[2048]{0:T(1024)} %param.21) | copy-start | bytes 24580
Sparse Core Ops, SparseCore 0:
  10.9 56.3 all-gather.6
  97.6 24.3 all-gather.10
  126.0 39.0 all-gather.8
where the time goes:
time: 205 us
  waiting for transfers between devices  84.8 us (41%)
  blocking collectives  40.6 us (20%)
  matrix products  27.4 us (13%)
  other arithmetic  20.4 us (10%)
  between operations  18 us (9%)
  local copies, waits for them, and re-layouts  13.3 us (6%)
    all_gather x1, waiting for transfers between devices, body(): lax.all_gather(normed, 'tp', axis=1, tiled=True)  53.8 us
    all_gather x2, waiting for transfers between devices, entering(): pieces = jax.tree.map(lambda part: lax.all_gather(part, axis), running)  30.9 us
    unnamed x2, blocking collectives  22.3 us
    all_to_all x1, blocking collectives, body(): lax.all_to_all(gated, 'tp', split_axis=1, concat_axis=2, tiled=True)  18.3 us
    dot_general x1, matrix products, body(): jnp.einsum('kux,xt->kut', lax.all_gather(normed, 'tp', axis=1, tiled=True...  9.51 us
    dot_general x1, matrix products, read_out(): jnp.einsum('shld,shdv->shlv', queries.astype(jnp.float32) * read_scale, c...  7.93 us
    unnamed x41, local copies, waits for them, and re-layouts  6.03 us
  transfers between devices with their start and end apart: 3, of which 3 were waited for; matrix products, arithmetic and copies ran while one was open for 4% of the time, Pallas kernels for 0%

commit v1 on v0

--- a/solution.py
+++ b/solution.py
@@ -11,6 +11,13 @@
 rms_eps = 1e-06
 group_eps = 1e-05
 rope_base = 10000.0
+
+
+def trade_parts(x, mesh_axis, split, join):
+    size = lax.axis_size(mesh_axis)
+    shards = jnp.stack(jnp.split(x, size, axis=split), axis=0)
+    shards = lax.all_to_all(shards, mesh_axis, split_axis=0, concat_axis=0)
+    return jnp.concatenate(shards, axis=join)
 
 
 def neutral_like(shard, identity):
@@ -159,7 +166,7 @@
     gated = (normal * norm_gain * jax.nn.silu(gating.astype(jnp.float32))).astype(jnp.bfloat16)
     premix = jnp.einsum(
         "hor,rn->hon",
-        lax.all_to_all(gated, "tp", split_axis=1, concat_axis=2, tiled=True),
+        trade_parts(gated, "tp", 1, 2),
         out_weight,
         preferred_element_type=jnp.float32,
     )

time: 205 us -> 197 us (0.961)
  local copies, waits for them, and re-layouts: 13.3 us -> 5.68 us
  matrix products: 27.4 us -> 24.5 us
    concatenate x8 -> x0, local copies, waits for them, and re-layouts: 2.8 us -> none  [rotate(): jnp.concatenate([first_half * cosine - second * sine_part, first_half * s...]
    unnamed x41 -> x40, local copies, waits for them, and re-layouts: 6.03 us -> 3.59 us
    dot_general x1, matrix products: 3.57 us -> 1.34 us  [body(): jnp.einsum('hor,rn->hon', trade_parts(gated, 'tp', 1, 2), out_weight, pre...]
where the time goes in v1:
time: 197 us
  waiting for transfers between devices  85.5 us (43%)
  blocking collectives  40.4 us (21%)
  matrix products  24.5 us (12%)
  other arithmetic  22.4 us (11%)
  between operations  18 us (9%)
  local copies, waits for them, and re-layouts  5.68 us (3%)
    all_gather x1, waiting for transfers between devices, body(): lax.all_gather(normed, 'tp', axis=1, tiled=True)  54.7 us
    all_gather x2, waiting for transfers between devices, entering(): pieces = jax.tree.map(lambda part: lax.all_gather(part, axis), running)  30.7 us
    unnamed x2, blocking collectives  22.1 us
    all_to_all x1, blocking collectives, trade_parts(): shards = lax.all_to_all(shards, mesh_axis, split_axis=0, concat_axis=0)  18.3 us
    dot_general x1, matrix products, body(): jnp.einsum('kux,xt->kut', lax.all_gather(normed, 'tp', axis=1, tiled=True...  8.43 us
    dot_general x1, matrix products, read_out(): jnp.einsum('shld,shdv->shlv', queries.astype(jnp.float32) * read_scale, c...  8.33 us
  transfers between devices with their start and end apart: 3, of which 3 were waited for; matrix products, arithmetic and copies ran while one was open for 4% of the time, Pallas kernels for 0%

profile of v1, /device:TPU:1, one launch (start us, length us, event | category | flops | bytes accessed | tf_op | source)
XLA Modules:
  0.0 196.6 jit_solution(126385107892916549)
XLA Ops:
  6.5 1.5 fusion.44
  8.1 2.7 %fusion.46 = bf16[4,64,2048]{2,1,0:T(8,128)(2,1)} fusion(bf16[4,64,2048]{2,1,0:T(8,128)(2,1)} %param.12, f32[2048]{0:T(1024)} %param.13, f32[4,64]{1,0:T(4,128)S(1)} %add_rsqrt_fusion.2), kind=kLoop, calls=%fused_computation.48 | loop fusion | flops 2097152 | bytes 2106368 | tf_op jit(solution)/shard_map/convert_element_type | solution.py:133
  11.7 1.0 multiply_cosine_fusion
  12.6 54.7 %all-gather.7.cloned.1.call-done = bf16[4,512,2048]{2,1,0:T(8,128)(2,1)} async-done(((bf16[4,64,2048]{2,1,0:T(8,128)(2,1)}), bf16[4,512,2048]{2,1,0:T(8,128)(2,1)}) %all-gather.7.cloned.1.call-update) | async-done | bytes 8388624 | tf_op jit(solution)/shard_map/all_gather | solution.py:137
  67.4 8.4 %fusion.54 = bf16[4,512,512]{2,1,0:T(8,128)(2,1)S(1)} fusion(bf16[4,512,2048]{2,1,0:T(8,128)(2,1)} %all-gather.7.cloned.1.call-done, bf16[2048,128]{1,0:T(8,128)(2,1)S(1)} %copy-done.8, bf16[2048,128]{1,0:T(8,128)(2,1)S(1)} %copy-done.9, bf16[2048,128]{1,0:T(8,128)(2,1)S(1)} %copy-done.10, bf16[2048,128]{1,0:T(8,128)(2,1)S(1)} %copy-done.11), kind=kOutput, calls=%fused_computation.59 | convolution fusion | flops 4304404480 | bytes 12582912 | tf_op jit(solution)/shard_map/kux,xt->kut/dot_general | solution.py:135
  76.2 0.8 fusion.58
  77.9 11.9 %while.15 = (s32[]{:T(128)}, f32[4,1,128,128]{3,2,0,1:T(8,128)S(1)}, f32[4,4,1,128,128]{4,3,1,2,0:T(8,128)}, f32[1]{0:T(128)}, bf16[4,4,1,128,128]{4,3,1,2,0:T(8...) while((s32[]{:T(128)}, ...), condition=%wide.region_2.3_spmd.clone.clone.clone, body=%wide.region_1.2_spmd.clone.clone.clone.sunk | while | flops 67977728 | bytes 2496632 | solution.py:87
  79.6 0.9 fusion.156
  82.6 0.9 fusion.156
  85.6 0.9 fusion.156
  88.5 0.9 fusion.156
  92.0 8.4 %all-reduce = f32[4]{0:T(128)S(1)} all-reduce(f32[4]{0:T(128)S(1)} %exponential_dynamic-update-slice_fusion), channel_id=2, replica_groups=mesh['sp_0'=8,'sp_1'=4,'tp'=8] {'sp_1'}, use_global_device_ids=true, to_apply=%add | all-reduce | flops 4 | bytes 32
  101.1 1.3 slice_multiply_fusion
  103.0 12.1 %all-gather.11.cloned.1.call-done = f32[16,1,128,128]{3,2,1,0:T(8,128)} async-done(((f32[4,1,128,128]{3,2,1,0:T(8,128)}), f32[16,1,128,128]{3,2,1,0:T(8,128)}) %all-gather.11.cloned.1.call-update) | async-done | bytes 1048592 | tf_op jit(solution)/shard_map/all_gather | solution.py:34
  115.1 3.8 %slice_add_fusion.8 = f32[4,1,128,128]{3,2,1,0:T(8,128)} fusion(f32[16,1,128,128]{3,2,1,0:T(8,128)} %all-gather.11.cloned.1.call-done, f32[]{:T(128)} %bitcast.26, f32[]{:T(128)} %bitcast.24, f32[16,1,128,128]{3,2,0,1:T(8,128)} %bitcast.223, f32[]{:T(128)} %bitcast.22, f32[]{:T(128)} %bitcast.19), kind=kLoop, calls=%fused_computation.114 | loop fusion | flops 458752 | bytes 1310736 | tf_op jit(solution)/shard_map/add | solution.py:99
  119.5 1.4 dynamic-update-slice.1
  120.9 13.7 %all-reduce.1 = f32[8]{0:T(128)S(1)} all-reduce(f32[8]{0:T(128)S(1)} %dynamic-update-slice.1), channel_id=3, replica_groups=mesh['sp_0'=8,'sp_1'=4,'tp'=8] {'sp_0'}, use_global_device_ids=true, to_apply=%add.1 | all-reduce | flops 8 | bytes 64
  138.5 1.0 copy.30
  139.6 18.6 %all-gather.9.cloned.1.call-done = f32[8,4,1,128,128]{4,3,2,1,0:T(8,128)} async-done(((f32[1,4,1,128,128]{4,3,2,1,0:T(8,128)}), f32[8,4,1,128,128]{4,3,2,1,0:T(8,128)}) %all-gather.9.cloned.1.call-update) | async-done | bytes 2097168 | tf_op jit(solution)/shard_map/all_gather | solution.py:34
  158.2 8.3 %fusion.136 = (f32[4,512]{1,0:T(4,128)S(1)}, f32[4,512,128]{2,1,0:T(8,128)S(1)}) fusion(f32[4,512,128]{2,1,0:T(8,128)} %bitcast.227, f32[8,4,1,128,128]{4,3,1,2,0:T(8,128)} %bitcast.228, f32[4,1,128,128]{3,2,1,0:T(8,128)S(1)} %copy-done.3, f32[16,1,128,128]{3,2,0,1:T(8,128)S(1)} %bitcast.224, f32[16,1,128,128]{3,2,1,0:T(8,128)S(1)} %copy-done.2, ...), kind=kOutput, calls=%fused_computation.194 | convolution fusion | flops 71170048 | bytes 6301756 | tf_op jit(solution)/shard_map/shld,shdv->shlv/dot_general | solution.py:108
  167.2 1.9 fusion.68
  169.2 18.3 %all_to_all.5 = bf16[8,4,64,128]{3,2,1,0:T(8,128)(2,1)S(1)} all-to-all(bf16[8,4,64,128]{3,2,1,0:T(8,128)(2,1)S(1)} %fusion.124), channel_id=1, replica_groups=mesh['sp_0'=8,'sp_1'=4,'tp'=8] {'tp'}, dimensions={0} | all-to-all | bytes 1048576 | tf_op jit(solution)/shard_map/all_to_all | solution.py:19
  187.5 1.3 multiply_reduce_fusion
  188.9 1.2 multiply_convert_fusion.2
  (78 shorter events, 14.1 us)
Async XLA Ops:
  6.5 60.9 %all-gather.7.cloned.1.call-start = ((), (), s32[]{:S(2)}) async-start(), calls=%async_computation.1 | async-start | bytes 9437184 | tf_op jit(solution)/shard_map/all_gather | solution.py:137
  8.1 59.3 %copy-start.8 = (bf16[2048,128]{1,0:T(8,128)(2,1)S(1)}, bf16[2048,128]{1,0:T(8,128)(2,1)}, u32[]{:S(2)}) copy-start(bf16[2048,128]{1,0:T(8,128)(2,1)} %param.17) | copy-start | bytes 1572868
  8.1 59.3 %copy-start.9 = (bf16[2048,128]{1,0:T(8,128)(2,1)S(1)}, bf16[2048,128]{1,0:T(8,128)(2,1)}, u32[]{:S(2)}) copy-start(bf16[2048,128]{1,0:T(8,128)(2,1)} %param.16) | copy-start | bytes 1572868
  8.1 59.3 %copy-start.10 = (bf16[2048,128]{1,0:T(8,128)(2,1)S(1)}, bf16[2048,128]{1,0:T(8,128)(2,1)}, u32[]{:S(2)}) copy-start(bf16[2048,128]{1,0:T(8,128)(2,1)} %param.15) | copy-start | bytes 1572868
  8.1 59.3 %copy-start.11 = (bf16[2048,128]{1,0:T(8,128)(2,1)S(1)}, bf16[2048,128]{1,0:T(8,128)(2,1)}, u32[]{:S(2)}) copy-start(bf16[2048,128]{1,0:T(8,128)(2,1)} %param.14) | copy-start | bytes 1572868
  10.9 104.3 %all-gather.11.cloned.1.call-start = ((), (), s32[]{:S(2)}) async-start(), calls=%async_computation.3 | async-start | bytes 1310720 | tf_op jit(solution)/shard_map/all_gather | solution.py:34
  75.8 1.3 copy-start.1
  77.9 12.8 %copy-start.13 = (u32[256]{0:T(256)S(1)}, u32[256]{0:T(256)}, u32[]{:S(2)}) copy-start(u32[256]{0:T(256)} %constant.86) | copy-start | bytes 3076
  77.9 41.1 %copy-start.12 = (u32[256]{0:T(256)S(1)}, u32[256]{0:T(256)}, u32[]{:S(2)}) copy-start(u32[256]{0:T(256)} %constant.91) | copy-start | bytes 3076
  89.8 0.7 copy-start
  89.8 48.7 %copy-start.4 = (f32[4,4,1,128,128]{4,3,1,2,0:T(8,128)S(1)}, f32[4,4,1,128,128]{4,3,1,2,0:T(8,128)}, u32[]{:S(2)}) copy-start(f32[4,4,1,128,128]{4,3,1,2,0:T(8,128)} %get-tuple-element.58) | copy-start | bytes 3145732
  90.6 67.6 %all-gather.9.cloned.1.call-start = ((), (), s32[]{:S(2)}) async-start(), calls=%async_computation.2 | async-start | bytes 2359296 | tf_op jit(solution)/shard_map/all_gather | solution.py:34
  115.1 43.1 %copy-start.2 = (f32[16,1,128,128]{3,2,1,0:T(8,128)S(1)}, f32[16,1,128,128]{3,2,1,0:T(8,128)}, u32[]{:S(2)}) copy-start(f32[16,1,128,128]{3,2,1,0:T(8,128)} %all-gather.11.cloned.1.call-done) | copy-start | bytes 3145732
  118.9 39.3 %copy-start.3 = (f32[4,1,128,128]{3,2,1,0:T(8,128)S(1)}, f32[4,1,128,128]{3,2,1,0:T(8,128)}, u32[]{:S(2)}) copy-start(f32[4,1,128,128]{3,2,1,0:T(8,128)} %slice_add_fusion.8) | copy-start | bytes 786436
  158.2 9.0 %copy-start.6 = (f32[128]{0:T(128)S(1)}, f32[128]{0:T(128)}, u32[]{:S(2)}) copy-start(f32[128]{0:T(128)} %param.19) | copy-start | bytes 1540
  167.2 20.3 %copy-start.7 = (bf16[1024,2048]{1,0:T(8,128)(2,1)S(1)}, bf16[1024,2048]{1,0:T(8,128)(2,1)}, u32[]{:S(2)}) copy-start(bf16[1024,2048]{1,0:T(8,128)(2,1)} %param.20) | copy-start | bytes 12582916
  187.5 1.4 copy-start.5
Sparse Core Ops, SparseCore 0:
  11.0 56.3 all-gather.6
  90.7 24.3 all-gather.10
  119.1 39.0 all-gather.8
